TPU v7x, 128 devices: a whole 4x4x4 slice. The times are simulated.
128 devices in a mesh: sp: 16 (over z, y), tp: 8 (over x, core).
Axes of the slice: x: 4, y: 4, z: 4, core: 2. Of those that a mesh axis runs over, the one named last changes fastest.
Arguments:
- tokens: bfloat16 [32768, 2048], P('sp'), may hold values from -6 to 6
- w_query: bfloat16 [2048, 1024], P(None, 'tp'), may hold values from -0.125 to 0.125
- w_key: bfloat16 [2048, 1024], P(None, 'tp'), may hold values from -0.125 to 0.125
- w_value: bfloat16 [2048, 1024], P(None, 'tp'), may hold values from -0.125 to 0.125
- w_gate: bfloat16 [2048, 1024], P(None, 'tp'), may hold values from -0.125 to 0.125
- w_pool: bfloat16 [2048, 1024], P(None, 'tp'), may hold values from -0.125 to 0.125
- norm_gain: float32 [1024], P('tp'), may hold values from 0.1 to 1.9
- log_decay: float32 [8, 32768], P('tp', 'sp'), may hold values from -0.8 to 0
- w_out: bfloat16 [2048, 2048], replicated, may hold values from -0.125 to 0.125
Outputs:
- mixed_out: bfloat16 [32768, 2048], P(('sp', 'tp'))
All inputs are finite; a program needn't handle non-finite values.
Results may differ from a plain program's by a relative error of at most 0.014.
Values may be sent and summed in bfloat16 or wider, within the bound.
A program may use at most 64 MiB of HBM per device.

v0:
```python
import jax
import jax.numpy as jnp
from jax import lax
from jax.sharding import PartitionSpec as P

HEAD_DIM = 128
POOL_GROUP = 256
BLOCK = 128
RET_WIDTH = 1024


def passed_along(block, axis, distance):
    devices = range(lax.axis_size(axis))
    route = [(i - distance, i) for i in devices if i - distance in devices]
    return lax.ppermute(block, axis, route)


def from_everyone(array, axis):
    peers = lax.axis_size(axis)
    return lax.all_to_all(
        jnp.broadcast_to(array[None], (peers, *array.shape)), axis, 0, 0, tiled=True
    )


def collected_together(array, axis):
    leaves = jax.tree.leaves(array)
    order = sorted(range(len(leaves)), key=lambda k: -leaves[k].size)
    width = (1, *leaves[order[0]].shape)[-1]
    lines = [
        jnp.pad(leaves[k].reshape(-1), (0, -leaves[k].size % width)).reshape(-1, width)
        for k in order
    ]
    both, at, found = (from_everyone(jnp.concatenate(lines), axis), 0, {})
    for k, line in zip(order, lines):
        share = both[:, at : at + len(line)].reshape(len(both), -1)
        found[k] = share[:, : leaves[k].size].reshape(-1, *leaves[k].shape)
        at += len(line)
    numbers = iter(range(len(leaves)))
    return jax.tree.map(lambda _: found[next(numbers)], array)


def folded_in_pairs(pieces, combine):
    while len(jax.tree.leaves(pieces)[0]) > 1:
        pieces = jax.vmap(combine)(
            *(jax.tree.map(lambda part: part[side::2], pieces) for side in (0, 1))
        )
    return jax.tree.map(lambda part: part[0], pieces)


def carried_in(array, axis, combine, identity):
    peers, here = (lax.axis_size(axis), lax.axis_index(axis))
    passed = jnp.arange(peers) < here

    def kept(part, zero, own):
        part = jnp.where(
            passed.reshape(-1, *(1 for _ in own.shape)), part, jnp.asarray(zero, own.dtype)
        )
        return part

    pieces = collected_together(array, axis)
    return folded_in_pairs(jax.tree.map(kept, pieces, identity, array), combine)


def rotate(tensor, positions):
    half_dim = tensor.shape[-1] // 2
    inverse = 10000.0 ** (-jnp.arange(half_dim, dtype=jnp.float32) / half_dim)
    angles = positions.astype(jnp.float32)[:, None] * inverse[None, :]
    cosine = jnp.cos(angles)[:, None, :]
    sine_part = jnp.sin(angles)[:, None, :]
    first_half = tensor[..., :half_dim]
    second_half = tensor[..., half_dim:]
    return jnp.concatenate(
        [
            first_half * cosine - second_half * sine_part,
            first_half * sine_part + second_half * cosine,
        ],
        axis=-1,
    )


def block_parts(q_blocks, k_blocks, v_blocks, decay_blocks):
    log_cum = jnp.cumsum(decay_blocks, axis=1)
    block_ends = log_cum[:, -1, :]
    steps_len = q_blocks.shape[1]
    causal = jnp.arange(steps_len)[:, None] >= jnp.arange(steps_len)[None, :]
    head_cum = jnp.transpose(log_cum, (0, 2, 1))
    log_gap = head_cum[:, :, :, None] - head_cum[:, :, None, :]
    weights = jnp.where(causal[None, None], jnp.exp(jnp.minimum(log_gap, 0.0)), 0.0)
    scores = jnp.einsum("nthd,nshd->nhts", q_blocks, k_blocks, preferred_element_type=jnp.float32)
    mixing = (scores * weights).astype(jnp.bfloat16)
    inner_part = jnp.einsum("nhts,nshe->nthe", mixing, v_blocks, preferred_element_type=jnp.float32)
    keys_decayed = (
        k_blocks.astype(jnp.float32) * jnp.exp(block_ends[:, None, :] - log_cum)[..., None]
    ).astype(jnp.bfloat16)
    updates = jnp.einsum(
        "nshd,nshe->nhde", keys_decayed, v_blocks, preferred_element_type=jnp.float32
    )
    return (log_cum, block_ends, inner_part, updates)


def chain_states(earlier, later):
    return (earlier[0] * later[0], earlier[1] * later[0][:, None, None] + later[1])


def local(tokens, w_query, w_key, w_value, w_gate, w_pool, norm_gain, log_decay, w_out):
    tok_rows = tokens.shape[0]
    n_heads = w_query.shape[1] // HEAD_DIM
    seq_index = lax.axis_index("sp")
    head_index = lax.axis_index("tp")

    def project(weights):
        return jnp.dot(tokens, weights, preferred_element_type=jnp.float32).astype(jnp.bfloat16)

    query = project(w_query)
    keys_raw = project(w_key)
    values = project(w_value)
    gate_pre = project(w_gate)
    pool_in = project(w_pool)
    rim_rows = passed_along(pool_in[tok_rows - 15 :], "sp", 1)
    positions = seq_index * tok_rows + jnp.arange(tok_rows)
    head_shape = (tok_rows, n_heads, HEAD_DIM)
    q_rot = rotate(query.astype(jnp.float32).reshape(head_shape), positions).astype(jnp.bfloat16)
    k_rot = (
        rotate(keys_raw.astype(jnp.float32).reshape(head_shape), positions) * HEAD_DIM ** (-0.5)
    ).astype(jnp.bfloat16)
    n_blocks = tok_rows // BLOCK
    block_shape = (n_blocks, BLOCK, n_heads, HEAD_DIM)
    q_blocks = q_rot.reshape(block_shape)
    k_blocks = k_rot.reshape(block_shape)
    v_blocks = values.reshape(block_shape)
    decay_blocks = jnp.transpose(log_decay).reshape(n_blocks, BLOCK, n_heads)
    log_cum, block_ends, inner_part, updates = block_parts(
        q_blocks, k_blocks, v_blocks, decay_blocks
    )

    def advance(running, element):
        block_end, update_n = element
        return (running * jnp.exp(block_end)[:, None, None] + update_n, running)

    zero_state = jnp.zeros((n_heads, HEAD_DIM, HEAD_DIM), jnp.float32)
    final_local, before_local = lax.scan(advance, zero_state, (block_ends, updates))
    end_cum = jnp.cumsum(block_ends, axis=0)
    dev_total = jnp.exp(end_cum[-1])
    reach = jnp.exp(end_cum - block_ends)
    identity = (jnp.ones_like(dev_total), jnp.zeros_like(final_local))
    _, incoming = carried_in((dev_total, final_local), "sp", chain_states, identity)
    before_state = before_local + reach[:, :, None, None] * incoming[None]
    state_bf = before_state.astype(jnp.bfloat16)
    cross_part = (
        jnp.einsum("nthd,nhde->nthe", q_blocks, state_bf, preferred_element_type=jnp.float32)
        * jnp.exp(log_cum)[..., None]
    )
    retained = (inner_part + cross_part).reshape(head_shape)
    centered = retained - jnp.mean(retained, axis=-1, keepdims=True)
    normed = centered * lax.rsqrt(jnp.mean(centered * centered, axis=-1, keepdims=True) + 1e-06)
    ret_cols = n_heads * HEAD_DIM
    gated = (
        jax.nn.silu(gate_pre.astype(jnp.float32)) * norm_gain * normed.reshape(tok_rows, ret_cols)
    ).astype(jnp.bfloat16)
    pool_cols = pool_in.shape[1]
    extended = jnp.concatenate([rim_rows, pool_in], axis=0).astype(jnp.float32)
    prefix = jnp.concatenate(
        [jnp.zeros((1, pool_cols), jnp.float32), jnp.cumsum(extended, axis=0)], axis=0
    )
    col_group = (head_index * pool_cols + jnp.arange(pool_cols)) // POOL_GROUP
    counts_base = (positions + 1).astype(jnp.float32)[:, None]
    upper_sum = prefix[16 : 16 + tok_rows]
    selected = jnp.zeros((tok_rows, pool_cols), jnp.float32)
    for group_idx in range(4):
        window_len = 2 ** (group_idx + 1)
        window_mean = (
            upper_sum - prefix[16 - window_len : 16 - window_len + tok_rows]
        ) / jnp.minimum(counts_base, float(window_len))
        selected = jnp.where((col_group == group_idx)[None, :], window_mean, selected)
    pooled = (selected - pool_in.astype(jnp.float32)).astype(jnp.bfloat16)
    ret_rows, pool_rows = (
        lax.all_to_all(gated, "tp", split_axis=0, concat_axis=1, tiled=True),
        lax.all_to_all(pooled, "tp", split_axis=0, concat_axis=1, tiled=True),
    )
    result = jnp.dot(ret_rows, w_out[:RET_WIDTH], preferred_element_type=jnp.float32) + jnp.dot(
        pool_rows, w_out[RET_WIDTH:], preferred_element_type=jnp.float32
    )
    return result.astype(jnp.bfloat16)


def solution(mesh):
    in_specs = (
        P("sp", None),
        P(None, "tp"),
        P(None, "tp"),
        P(None, "tp"),
        P(None, "tp"),
        P(None, "tp"),
        P("tp"),
        P("tp", "sp"),
        P(),
    )
    out_specs = P(("sp", "tp"), None)
    return jax.shard_map(local, mesh=mesh, in_specs=in_specs, out_specs=out_specs, check_vma=False)
```

profile of v0, /device:TPU:32, one launch (start us, length us, event | category | flops | bytes accessed | tf_op | source)
XLA Modules:
  0.0 151.4 jit_solution(8528423157894096770)
XLA Ops:
  0.0 1.3 copy.38
  1.3 23.3 %fusion.77 = f32[16,128,1]{2,0,1:T(8,128)S(1)} fusion(f32[16,128,1]{2,0,1:T(8,128)S(1)} %copy.38), kind=kOutput, calls=%fused_computation.132 | output fusion | flops 260096 | bytes 16384 | tf_op jit(solution)/shard_map/jit(cumsum)/reduce_window_sum | solution.py:82
  25.2 6.3 %fusion.12 = f32[2048,1,128]{0,2,1:T(8,128)S(1)} fusion(bf16[2048,2048]{1,0:T(8,128)(2,1)} %param.11, bf16[2048,128]{1,0:T(8,128)(2,1)S(1)} %copy-done), kind=kOutput, calls=%fused_computation.16 | convolution fusion | flops 1074266112 | bytes 9961472 | tf_op jit(solution)/shard_map/dot_general | solution.py:112
  31.5 6.3 %fusion.14 = f32[2048,1,128]{0,2,1:T(8,128)S(1)} fusion(bf16[2048,2048]{1,0:T(8,128)(2,1)} %param.11, bf16[2048,128]{1,0:T(8,128)(2,1)S(1)} %copy-done.7), kind=kOutput, calls=%fused_computation.18 | convolution fusion | flops 1074266112 | bytes 9961472 | tf_op jit(solution)/shard_map/dot_general | solution.py:112
  37.8 3.0 %fusion.51 = (bf16[2048,1,64]{0,2,1:T(8,128)(2,1)}, bf16[2048,1,64]{0,2,1:T(8,128)(2,1)S(1)}, f32[2048,1,64]{0,2,1:T(8,128)S(1)}, f32[2048,1,64]{0,2,1:T(8,128)S(1)}) fusion(f32[2048,1,128]{0,2,1:T(8,128)S(1)} %fusion.12, f32[64]{0:T(128)S(1)} %multiply_power_fusion, f32[2048]{0:T(1024)S(1)} %fusion.67, f32[2048,1,128]{0,2,1:T(8,128)S(1)} %fusion.14), kind=kLoop, calls=%fused_computation.74 | loop fusion | flops 1966080 | bytes 3678464 | tf_op jit(solution)/shard_map/convert.9
  41.5 6.6 %convolution_convert_fusion.3 = bf16[2048,128]{1,0:T(8,128)(2,1)} fusion(bf16[2048,2048]{1,0:T(8,128)(2,1)} %param.11, bf16[2048,128]{1,0:T(8,128)(2,1)} %param.14), kind=kOutput, calls=%fused_computation.12 | convolution fusion | flops 1074003968 | bytes 9437184 | tf_op jit(solution)/shard_map/dot_general | solution.py:112
  49.9 32.1 %while.13 = (s32[]{:T(128)}, f32[1,128,128]{2,1,0:T(8,128)S(1)}, f32[16,1,128,128]{3,2,1,0:T(8,128)}, f32[16,1]{0,1:T(1,128)S(1)}, f32[16,1,128,128]{3,2,1,0:T(8,128)S(1)}, /*index=5*/s32[]{:T(128)}, s32[]{:T(128)}) while((s32[]{:T(128)}, f32[1,128,128]{2,1,0:T(8,128)S(1)}, f32[16,1,128,128]{3,2,1,0:T(8,128)}, ...), condition=%wide.region_2.3_spmd.clone, body=%wide.region_1.2_spmd.clone.sunk | while | flops 65539 | bytes 328300 | solution.py:141
  83.4 1.1 broadcast_in_dim.58
  84.5 8.1 %all-to-all-start = ((f32[16,129,128]{2,1,0:T(8,128)}), f32[16,129,128]{2,1,0:T(8,128)}, u32[]{:S(2)}, u32[]{:S(2)}) async-start(f32[16,129,128]{2,1,0:T(8,128)} %broadcast_in_dim.58), calls=%async_computation | async-start | bytes 2228224 | tf_op jit(solution)/shard_map/all_to_all | solution.py:20
  92.6 5.8 %convolution_convert_fusion = bf16[2048,128]{1,0:T(8,128)(2,1)S(1)} fusion(bf16[2048,2048]{1,0:T(8,128)(2,1)} %param.11, bf16[2048,128]{1,0:T(8,128)(2,1)S(1)} %copy-done.8), kind=kOutput, calls=%fused_computation.9 | convolution fusion | flops 1074003968 | bytes 9437184 | tf_op jit(solution)/shard_map/dot_general | solution.py:112
  98.4 3.5 %collective-permute-start = (bf16[15,128]{1,0:T(8,128)(2,1)S(1)}, bf16[15,128]{1,0:T(8,128)(2,1)S(1)}, u32[]{:S(2)}, u32[]{:S(2)}) collective-permute-start(bf16[15,128]{1,0:T(8,128)(2,1)S(1)} %slice.158), channel_id=1, source_target_pairs={{0,8},{8,16},{16,24},{24,32},{32,40},{40,48},{48,56},{56,64},{64,7... | collective-permute-start | bytes 11528 | tf_op jit(solution)/shard_map/ppermute | solution.py:15
  103.5 3.4 %collective-permute-done = bf16[15,128]{1,0:T(8,128)(2,1)S(1)} collective-permute-done((bf16[15,128]{1,0:T(8,128)(2,1)S(1)}, bf16[15,128]{1,0:T(8,128)(2,1)S(1)}, u32[]{:S(2)}, u32[]{:S(2)}) %collective-permute-start) | collective-permute-done | bytes 3872 | tf_op jit(solution)/shard_map/ppermute | solution.py:15
  109.1 1.8 %fusion.41 = bf16[2048,128]{1,0:T(8,128)(2,1)S(1)} fusion(bf16[2048,128]{1,0:T(8,128)(2,1)S(1)} %copy-done.3, f32[2176,128]{1,0:T(8,128)S(1)} %bitcast.113, f32[2063,128]{1,0:T(8,128)S(1)} %slice.162, f32[2048]{0:T(1024)S(1)} %get-tuple-element.98, f32[2048]{0:T(1024)S(1)} %get-tuple-element.99, f32[2048]{0:T(1024)S(1)} %get-tuple-element.100, ...), kind=kLoop, calls=%fused_computation.60 | loop fusion | flops 3932160 | bytes 6332416 | tf_op jit(solution)/shard_map/convert_element_type | solution.py:175
  110.9 1.0 copy.46
  111.9 4.3 %all-to-all-start.2 = ((bf16[8,256,128]{1,2,0:T(8,128)(2,1)}), bf16[8,256,128]{1,2,0:T(8,128)(2,1)}, u32[]{:S(2)}, u32[]{:S(2)}) async-start(bf16[8,256,128]{1,2,0:T(8,128)(2,1)} %copy.46), calls=%async_computation.2 | async-start | bytes 1048576 | tf_op jit(solution)/shard_map/all_to_all | solution.py:178
  118.0 1.5 fusion.30
  120.4 1.6 %fusion.18 = f32[16,1,128,128]{2,3,0,1:T(8,128)} fusion(f32[16,1,128,128]{3,2,1,0:T(8,128)S(1)} %copy-done.5, f32[16,128]{1,0:T(8,128)S(1)} %get-tuple-element.88, f32[128,128]{1,0:T(8,128)S(1)} %fusion.65, f32[16]{0:T(128)S(1)} %subtract_exponential_fusion.1, bf16[16,128,64]{2,1,0:T(8,128)(2,1)S(1)} %bitcast.117, bf16[16,128,64]{2,1,0:T(8,128)(2,1)S(1)} %bitcast.115), kind=kOutput, calls=%fused_computation.26 | convolution fusion | flops 69206016 | bytes 2695232 | tf_op jit(solution)/shard_map/nthd,nhde->nthe/dot_general | solution.py:150
  122.0 2.3 %bitcast_reduce_fusion = (f32[16,128]{1,0:T(8,128)S(1)}, f32[16,1,128,128]{2,3,0,1:T(8,128)S(1)}) fusion(f32[16,1,128,128]{2,3,0,1:T(8,128)} %fusion.18, bf16[16,128,128]{2,1,0:T(8,128)(2,1)} %bitcast.123, bf16[16,128,128]{2,1,0:T(8,128)(2,1)S(1)} %fusion.31, f32[16,128]{1,0:T(8,128)S(1)} %bitcast.127, pred[128,128]{1,0:T(8,128)(4,1)S(1)} %iota_compare_fusion, ...), kind=kOutput, calls=%fused_computation.50 | convolution fusion | flops 137099264 | bytes 3702784 | tf_op jit(solution)/shard_map/nhts,nshe->nthe/dot_general | solution.py:91
  125.0 5.9 %fusion.34 = bf16[2048,128]{1,0:T(8,128)(2,1)S(1)} fusion(f32[16,1,128,128]{2,3,0,1:T(8,128)S(1)} %get-tuple-element.97, bf16[2048,2048]{1,0:T(8,128)(2,1)} %param.11, bf16[2048,128]{1,0:T(8,128)(2,1)} %param.15, f32[2048]{0:T(1024)S(1)} %rsqrt_bitcast_fusion, f32[2048]{0:T(1024)S(1)} %get-tuple-element.86, f32[128]{0:T(128)S(1)} %copy-done.9), kind=kOutput, calls=%fused_computation.49 | convolution fusion | flops 1076625408 | bytes 10502656 | tf_op jit(solution)/shard_map/dot_general | solution.py:112
  130.8 1.0 copy.43
  131.9 4.8 %all-to-all-start.1 = ((bf16[8,256,128]{1,2,0:T(8,128)(2,1)}), bf16[8,256,128]{1,2,0:T(8,128)(2,1)S(1)}, u32[]{:S(2)}, u32[]{:S(2)}) async-start(bf16[8,256,128]{1,2,0:T(8,128)(2,1)} %copy.43), calls=%async_computation.1 | async-start | bytes 1048576 | tf_op jit(solution)/shard_map/all_to_all | solution.py:177
  136.7 3.6 %fusion = f32[256,2048]{1,0:T(8,128)S(1)} fusion(bf16[256,1024]{0,1:T(8,128)(2,1)} %bitcast.39, bf16[2048,2048]{1,0:T(8,128)(2,1)} %param.19), kind=kOutput, calls=%fused_computation.3 | convolution fusion | flops 1073741824 | bytes 6815744 | tf_op jit(solution)/shard_map/dot_general | solution.py:180
  140.3 6.7 %all-to-all-done.1 = bf16[8,256,128]{1,2,0:T(8,128)(2,1)S(1)} async-done(((bf16[8,256,128]{1,2,0:T(8,128)(2,1)}), bf16[8,256,128]{1,2,0:T(8,128)(2,1)S(1)}, u32[]{:S(2)}, u32[]{:S(2)}) %all-to-all-start.1) | async-done | bytes 524320 | tf_op jit(solution)/shard_map/all_to_all | solution.py:177
  147.0 4.4 %fusion.7 = bf16[256,2048]{1,0:T(8,128)(2,1)} fusion(f32[256,2048]{1,0:T(8,128)S(1)} %fusion, bf16[256,1024]{0,1:T(8,128)(2,1)S(1)} %bitcast.125, bf16[2048,2048]{1,0:T(8,128)(2,1)} %param.19), kind=kOutput, calls=%fused_computation.8 | convolution fusion | flops 1074790400 | bytes 7864320 | tf_op jit(solution)/shard_map/dot_general | solution.py:180
  (124 shorter events, 42.3 us)
Async XLA Ops:
  0.0 25.2 %copy-start = (bf16[2048,128]{1,0:T(8,128)(2,1)S(1)}, bf16[2048,128]{1,0:T(8,128)(2,1)}, u32[]{:S(2)}) copy-start(bf16[2048,128]{1,0:T(8,128)(2,1)} %param.12) | copy-start | bytes 1572868
  25.2 6.4 %copy-start.7 = (bf16[2048,128]{1,0:T(8,128)(2,1)S(1)}, bf16[2048,128]{1,0:T(8,128)(2,1)}, u32[]{:S(2)}) copy-start(bf16[2048,128]{1,0:T(8,128)(2,1)} %param.13) | copy-start | bytes 1572868
  48.1 1.0 copy-start.4
  82.0 10.6 %copy-start.8 = (bf16[2048,128]{1,0:T(8,128)(2,1)S(1)}, bf16[2048,128]{1,0:T(8,128)(2,1)}, u32[]{:S(2)}) copy-start(bf16[2048,128]{1,0:T(8,128)(2,1)} %param.16) | copy-start | bytes 1572868
  84.5 27.4 %all-to-all-start = ((f32[16,129,128]{2,1,0:T(8,128)}), f32[16,129,128]{2,1,0:T(8,128)}, u32[]{:S(2)}, u32[]{:S(2)}) async-start(f32[16,129,128]{2,1,0:T(8,128)} %broadcast_in_dim.58), calls=%async_computation | async-start | bytes 2228224 | tf_op jit(solution)/shard_map/all_to_all | solution.py:20
  92.6 9.6 %copy-start.6 = (bf16[2048,1,64]{0,2,1:T(8,128)(2,1)S(1)}, bf16[2048,1,64]{0,2,1:T(8,128)(2,1)}, u32[]{:S(2)}) copy-start(bf16[2048,1,64]{0,2,1:T(8,128)(2,1)} %get-tuple-element.78) | copy-start | bytes 786436
  98.4 8.7 %copy-start.2 = (bf16[2048,128]{1,0:T(8,128)(2,1)}, bf16[2048,128]{1,0:T(8,128)(2,1)S(1)}, u32[]{:S(2)}) copy-start(bf16[2048,128]{1,0:T(8,128)(2,1)S(1)} %convolution_convert_fusion) | copy-start | bytes 1572868
  98.4 8.5 %collective-permute-start = (bf16[15,128]{1,0:T(8,128)(2,1)S(1)}, bf16[15,128]{1,0:T(8,128)(2,1)S(1)}, u32[]{:S(2)}, u32[]{:S(2)}) collective-permute-start(bf16[15,128]{1,0:T(8,128)(2,1)S(1)} %slice.158), channel_id=1, source_target_pairs={{0,8},{8,16},{16,24},{24,32},{32,40},{40,48},{48,56},{56,64},{64,7... | collective-permute-start | bytes 11528 | tf_op jit(solution)/shard_map/ppermute | solution.py:15
  108.1 1.0 copy-start.3
  111.9 19.9 %all-to-all-start.2 = ((bf16[8,256,128]{1,2,0:T(8,128)(2,1)}), bf16[8,256,128]{1,2,0:T(8,128)(2,1)}, u32[]{:S(2)}, u32[]{:S(2)}) async-start(bf16[8,256,128]{1,2,0:T(8,128)(2,1)} %copy.46), calls=%async_computation.2 | async-start | bytes 1048576 | tf_op jit(solution)/shard_map/all_to_all | solution.py:178
  118.0 2.4 %copy-start.1 = (bf16[2048,1,64]{2,0,1:T(8,128)(2,1)S(1)}, bf16[2048,1,64]{2,0,1:T(8,128)(2,1)}, u32[]{:S(2)}) copy-start(bf16[2048,1,64]{2,0,1:T(8,128)(2,1)} %copy.49) | copy-start | bytes 786436
  118.0 2.4 %copy-start.5 = (f32[16,1,128,128]{3,2,1,0:T(8,128)S(1)}, f32[16,1,128,128]{3,2,1,0:T(8,128)}, u32[]{:S(2)}) copy-start(f32[16,1,128,128]{3,2,1,0:T(8,128)} %get-tuple-element.33) | copy-start | bytes 3145732
  122.0 3.0 %copy-start.9 = (f32[128]{0:T(128)S(1)}, f32[128]{0:T(128)}, u32[]{:S(2)}) copy-start(f32[128]{0:T(128)} %param.17) | copy-start | bytes 1540
  131.9 15.1 %all-to-all-start.1 = ((bf16[8,256,128]{1,2,0:T(8,128)(2,1)}), bf16[8,256,128]{1,2,0:T(8,128)(2,1)S(1)}, u32[]{:S(2)}, u32[]{:S(2)}) async-start(bf16[8,256,128]{1,2,0:T(8,128)(2,1)} %copy.43), calls=%async_computation.1 | async-start | bytes 1048576 | tf_op jit(solution)/shard_map/all_to_all | solution.py:177
where the time goes:
time: 152 us; the launch traced here: 151 us
  other arithmetic  54.5 us (36%)
  matrix products  43.5 us (29%)
  local copies, waits for them, and re-layouts  21.1 us (14%)
  starting transfers between devices  20.7 us (14%)
  waiting for transfers between devices  10.1 us (7%)
    dot_general x5, matrix products, project(): jnp.dot(tokens, weights, preferred_element_type=jnp.float32)  30.8 us
    another operation x1, other arithmetic, block_parts(): log_cum = jnp.cumsum(decay_blocks, axis=1)  23.3 us
    add x16, other arithmetic, advance(): return (running * jnp.exp(block_end)[:, None, None] + update_n, running)  11 us
    exp x16, local copies, waits for them, and re-layouts, advance(): return (running * jnp.exp(block_end)[:, None, None] + update_n, running)  10.5 us
    dynamic_update_slice x16, other arithmetic, local(): lax.scan(advance, zero_state, (block_ends, updates))  10.3 us
    all_to_all x1, starting transfers between devices, from_everyone(): lax.all_to_all(jnp.broadcast_to(array[None], (peers, *array.shape)), axis...  8.07 us
    all_to_all x1, waiting for transfers between devices, local(): lax.all_to_all(gated, 'tp', split_axis=0, concat_axis=1, tiled=True)  6.69 us
    all_to_all x1, starting transfers between devices, local(): lax.all_to_all(gated, 'tp', split_axis=0, concat_axis=1, tiled=True)  4.8 us
  transfers between devices with their start and end apart: 4, of which 2 were waited for; matrix products, arithmetic and copies ran while one was open for 20% of the time, Pallas kernels for 0%

commit v1 on v0

--- a/solution.py
+++ b/solution.py
@@ -1,3 +1,4 @@
+import functools
 import jax
 import jax.numpy as jnp
 from jax import lax
@@ -7,6 +8,17 @@
 POOL_GROUP = 256
 BLOCK = 128
 RET_WIDTH = 1024
+
+
+def patch_pass(xx, bus_axis):
+    t1 = lax.axis_size(bus_axis)
+    q_next = jnp.split(xx, t1, 0)
+    u1 = jnp.stack(q_next, axis=0)
+    far_arr = lax.all_to_all(u1, bus_axis, split_axis=0, concat_axis=0)
+    return jnp.concatenate(far_arr, axis=1)
+
+
+_recover_desk = functools.partial(patch_pass, bus_axis="tp")
 
 
 def passed_along(block, axis, distance):
@@ -174,7 +186,7 @@
         selected = jnp.where((col_group == group_idx)[None, :], window_mean, selected)
     pooled = (selected - pool_in.astype(jnp.float32)).astype(jnp.bfloat16)
     ret_rows, pool_rows = (
-        lax.all_to_all(gated, "tp", split_axis=0, concat_axis=1, tiled=True),
+        _recover_desk(gated),
         lax.all_to_all(pooled, "tp", split_axis=0, concat_axis=1, tiled=True),
     )
     result = jnp.dot(ret_rows, w_out[:RET_WIDTH], preferred_element_type=jnp.float32) + jnp.dot(

time: 152 us -> 157 us (1.033)
  local copies, waits for them, and re-layouts: 21.1 us -> 25.4 us
  matrix products: 43.5 us -> 45.6 us
    unnamed x20 -> x27, local copies, waits for them, and re-layouts: 1.39 us -> 5.83 us
  transfers between devices with their start and end apart: 4 -> 4, of which waited for: 2 -> 2; matrix products, arithmetic and copies ran while one was open for 20% -> 23% of each run, Pallas kernels for 0% -> 0%
where the time goes in v1:
time: 157 us; the launch traced here: 156 us
  other arithmetic  54.5 us (35%)
  matrix products  45.6 us (29%)
  local copies, waits for them, and re-layouts  25.4 us (16%)
  starting transfers between devices  20.7 us (13%)
  waiting for transfers between devices  8.74 us (6%)
    dot_general x5, matrix products, project(): jnp.dot(tokens, weights, preferred_element_type=jnp.float32)  30.8 us
    another operation x1, other arithmetic, block_parts(): log_cum = jnp.cumsum(decay_blocks, axis=1)  23.3 us
    add x16, other arithmetic, advance(): return (running * jnp.exp(block_end)[:, None, None] + update_n, running)  11 us
    exp x16, local copies, waits for them, and re-layouts, advance(): return (running * jnp.exp(block_end)[:, None, None] + update_n, running)  10.5 us
    dynamic_update_slice x16, other arithmetic, local(): lax.scan(advance, zero_state, (block_ends, updates))  10.3 us
    all_to_all x1, starting transfers between devices, from_everyone(): lax.all_to_all(jnp.broadcast_to(array[None], (peers, *array.shape)), axis...  8.07 us
    unnamed x27, local copies, waits for them, and re-layouts  5.83 us
    all_to_all x1, waiting for transfers between devices, patch_pass(): far_arr = lax.all_to_all(u1, bus_axis, split_axis=0, concat_axis=0)  5.34 us
  transfers between devices with their start and end apart: 4, of which 2 were waited for; matrix products, arithmetic and copies ran while one was open for 23% of the time, Pallas kernels for 0%

profile of v1, /device:TPU:32, one launch (start us, length us, event | category | flops | bytes accessed | tf_op | source)
XLA Modules:
  0.0 156.4 jit_solution(2165020219627752205)
XLA Ops:
  0.0 1.3 copy.38
  1.3 23.3 %fusion.85 = f32[16,128,1]{2,0,1:T(8,128)S(1)} fusion(f32[16,128,1]{2,0,1:T(8,128)S(1)} %copy.38), kind=kOutput, calls=%fused_computation.148 | output fusion | flops 260096 | bytes 16384 | tf_op jit(solution)/shard_map/jit(cumsum)/reduce_window_sum | solution.py:94
  25.2 6.3 %fusion.12 = f32[2048,1,128]{0,2,1:T(8,128)S(1)} fusion(bf16[2048,2048]{1,0:T(8,128)(2,1)} %param.11, bf16[2048,128]{1,0:T(8,128)(2,1)S(1)} %copy-done), kind=kOutput, calls=%fused_computation.16 | convolution fusion | flops 1074266112 | bytes 9961472 | tf_op jit(solution)/shard_map/dot_general | solution.py:124
  31.5 6.3 %fusion.14 = f32[2048,1,128]{0,2,1:T(8,128)S(1)} fusion(bf16[2048,2048]{1,0:T(8,128)(2,1)} %param.11, bf16[2048,128]{1,0:T(8,128)(2,1)S(1)} %copy-done.7), kind=kOutput, calls=%fused_computation.18 | convolution fusion | flops 1074266112 | bytes 9961472 | tf_op jit(solution)/shard_map/dot_general | solution.py:124
  37.8 3.0 %fusion.51 = (bf16[2048,1,64]{0,2,1:T(8,128)(2,1)}, bf16[2048,1,64]{0,2,1:T(8,128)(2,1)S(1)}, f32[2048,1,64]{0,2,1:T(8,128)S(1)}, f32[2048,1,64]{0,2,1:T(8,128)S(1)}) fusion(f32[2048,1,128]{0,2,1:T(8,128)S(1)} %fusion.12, f32[64]{0:T(128)S(1)} %multiply_power_fusion, f32[2048]{0:T(1024)S(1)} %fusion.75, f32[2048,1,128]{0,2,1:T(8,128)S(1)} %fusion.14), kind=kLoop, calls=%fused_computation.74 | loop fusion | flops 1966080 | bytes 3678464 | tf_op jit(solution)/shard_map/convert.9
  41.5 6.6 %convolution_convert_fusion.3 = bf16[2048,128]{1,0:T(8,128)(2,1)} fusion(bf16[2048,2048]{1,0:T(8,128)(2,1)} %param.11, bf16[2048,128]{1,0:T(8,128)(2,1)} %param.14), kind=kOutput, calls=%fused_computation.12 | convolution fusion | flops 1074003968 | bytes 9437184 | tf_op jit(solution)/shard_map/dot_general | solution.py:124
  49.9 32.1 %while.13 = (s32[]{:T(128)}, f32[1,128,128]{2,1,0:T(8,128)S(1)}, f32[16,1,128,128]{3,2,1,0:T(8,128)}, f32[16,1]{0,1:T(1,128)S(1)}, f32[16,1,128,128]{3,2,1,0:T(8,128)S(1)}, /*index=5*/s32[]{:T(128)}, s32[]{:T(128)}) while((s32[]{:T(128)}, f32[1,128,128]{2,1,0:T(8,128)S(1)}, f32[16,1,128,128]{3,2,1,0:T(8,128)}, ...), condition=%wide.region_2.3_spmd.clone, body=%wide.region_1.2_spmd.clone.sunk | while | flops 65539 | bytes 328300 | solution.py:153
  83.4 1.1 broadcast_in_dim.58
  84.5 8.1 %all-to-all-start = ((f32[16,129,128]{2,1,0:T(8,128)}), f32[16,129,128]{2,1,0:T(8,128)}, u32[]{:S(2)}, u32[]{:S(2)}) async-start(f32[16,129,128]{2,1,0:T(8,128)} %broadcast_in_dim.58), calls=%async_computation | async-start | bytes 2228224 | tf_op jit(solution)/shard_map/all_to_all | solution.py:32
  92.6 5.8 %convolution_convert_fusion = bf16[2048,128]{1,0:T(8,128)(2,1)S(1)} fusion(bf16[2048,2048]{1,0:T(8,128)(2,1)} %param.11, bf16[2048,128]{1,0:T(8,128)(2,1)S(1)} %copy-done.8), kind=kOutput, calls=%fused_computation.9 | convolution fusion | flops 1074003968 | bytes 9437184 | tf_op jit(solution)/shard_map/dot_general | solution.py:124
  98.4 3.5 %collective-permute-start = (bf16[15,128]{1,0:T(8,128)(2,1)S(1)}, bf16[15,128]{1,0:T(8,128)(2,1)S(1)}, u32[]{:S(2)}, u32[]{:S(2)}) collective-permute-start(bf16[15,128]{1,0:T(8,128)(2,1)S(1)} %slice.158), channel_id=1, source_target_pairs={{0,8},{8,16},{16,24},{24,32},{32,40},{40,48},{48,56},{56,64},{64,7... | collective-permute-start | bytes 11528 | tf_op jit(solution)/shard_map/ppermute | solution.py:27
  102.5 1.0 copy.49
  103.5 3.4 %collective-permute-done = bf16[15,128]{1,0:T(8,128)(2,1)S(1)} collective-permute-done((bf16[15,128]{1,0:T(8,128)(2,1)S(1)}, bf16[15,128]{1,0:T(8,128)(2,1)S(1)}, u32[]{:S(2)}, u32[]{:S(2)}) %collective-permute-start) | collective-permute-done | bytes 3872 | tf_op jit(solution)/shard_map/ppermute | solution.py:27
  109.1 1.8 %fusion.41 = bf16[2048,128]{1,0:T(8,128)(2,1)S(1)} fusion(bf16[2048,128]{1,0:T(8,128)(2,1)S(1)} %copy-done.3, f32[2176,128]{1,0:T(8,128)S(1)} %bitcast.143, f32[2063,128]{1,0:T(8,128)S(1)} %slice.162, f32[2048]{0:T(1024)S(1)} %get-tuple-element.98, f32[2048]{0:T(1024)S(1)} %get-tuple-element.99, f32[2048]{0:T(1024)S(1)} %get-tuple-element.100, ...), kind=kLoop, calls=%fused_computation.60 | loop fusion | flops 3932160 | bytes 6332416 | tf_op jit(solution)/shard_map/convert_element_type | solution.py:187
  110.9 1.0 copy.46
  111.9 4.3 %all-to-all-start.2 = ((bf16[8,256,128]{1,2,0:T(8,128)(2,1)}), bf16[8,256,128]{1,2,0:T(8,128)(2,1)}, u32[]{:S(2)}, u32[]{:S(2)}) async-start(bf16[8,256,128]{1,2,0:T(8,128)(2,1)} %copy.46), calls=%async_computation.2 | async-start | bytes 1048576 | tf_op jit(solution)/shard_map/all_to_all | solution.py:190
  118.0 1.5 fusion.30
  120.4 1.6 %fusion.18 = f32[16,1,128,128]{2,3,0,1:T(8,128)} fusion(f32[16,1,128,128]{3,2,1,0:T(8,128)S(1)} %copy-done.5, f32[16,128]{1,0:T(8,128)S(1)} %get-tuple-element.88, f32[128,128]{1,0:T(8,128)S(1)} %fusion.73, f32[16]{0:T(128)S(1)} %subtract_exponential_fusion.1, bf16[16,128,64]{2,1,0:T(8,128)(2,1)S(1)} %bitcast.147, bf16[16,128,64]{2,1,0:T(8,128)(2,1)S(1)} %bitcast.145), kind=kOutput, calls=%fused_computation.26 | convolution fusion | flops 69206016 | bytes 2695232 | tf_op jit(solution)/shard_map/nthd,nhde->nthe/dot_general | solution.py:162
  122.0 2.3 %bitcast_reduce_fusion = (f32[16,128]{1,0:T(8,128)S(1)}, f32[16,1,128,128]{2,3,0,1:T(8,128)S(1)}) fusion(f32[16,1,128,128]{2,3,0,1:T(8,128)} %fusion.18, bf16[16,128,128]{2,1,0:T(8,128)(2,1)} %bitcast.154, bf16[16,128,128]{2,1,0:T(8,128)(2,1)S(1)} %fusion.31, f32[16,128]{1,0:T(8,128)S(1)} %bitcast.157, pred[128,128]{1,0:T(8,128)(4,1)S(1)} %iota_compare_fusion, ...), kind=kOutput, calls=%fused_computation.50 | convolution fusion | flops 137099264 | bytes 3702784 | tf_op jit(solution)/shard_map/nhts,nshe->nthe/dot_general | solution.py:103
  125.0 5.9 %fusion.34 = bf16[2048,128]{1,0:T(8,128)(2,1)S(1)} fusion(f32[16,1,128,128]{2,3,0,1:T(8,128)S(1)} %get-tuple-element.97, bf16[2048,2048]{1,0:T(8,128)(2,1)} %param.11, bf16[2048,128]{1,0:T(8,128)(2,1)} %param.15, f32[2048]{0:T(1024)S(1)} %rsqrt_bitcast_fusion, f32[2048]{0:T(1024)S(1)} %get-tuple-element.86, f32[128]{0:T(128)S(1)} %copy-done.9), kind=kOutput, calls=%fused_computation.49 | convolution fusion | flops 1076625408 | bytes 10502656 | tf_op jit(solution)/shard_map/dot_general | solution.py:124
  135.9 4.8 %all-to-all-start.1 = ((bf16[8,256,128]{2,1,0:T(8,128)(2,1)}), bf16[8,256,128]{2,1,0:T(8,128)(2,1)S(1)}, u32[]{:S(2)}, u32[]{:S(2)}) async-start(bf16[8,256,128]{2,1,0:T(8,128)(2,1)} %fusion.65), calls=%async_computation.1 | async-start | bytes 1048576 | tf_op jit(solution)/shard_map/all_to_all | solution.py:17
  140.7 5.0 %fusion = f32[256,2048]{1,0:T(8,128)} fusion(bf16[256,1024]{0,1:T(8,128)(2,1)} %bitcast.46, bf16[2048,2048]{1,0:T(8,128)(2,1)} %param.19), kind=kOutput, calls=%fused_computation.3 | convolution fusion | flops 1073741824 | bytes 6815744 | tf_op jit(solution)/shard_map/dot_general | solution.py:192
  145.7 5.3 %all-to-all-done.1 = bf16[8,256,128]{2,1,0:T(8,128)(2,1)S(1)} async-done(((bf16[8,256,128]{2,1,0:T(8,128)(2,1)}), bf16[8,256,128]{2,1,0:T(8,128)(2,1)S(1)}, u32[]{:S(2)}, u32[]{:S(2)}) %all-to-all-start.1) | async-done | bytes 524320 | tf_op jit(solution)/shard_map/all_to_all | solution.py:17
  151.3 5.1 %fusion.7 = bf16[256,2048]{1,0:T(8,128)(2,1)} fusion(f32[256,2048]{1,0:T(8,128)} %fusion, bf16[256,1024]{0,1:T(8,128)(2,1)S(1)} %bitcast.156, bf16[2048,2048]{1,0:T(8,128)(2,1)} %param.19), kind=kOutput, calls=%fused_computation.8 | convolution fusion | flops 1074790400 | bytes 7864320 | tf_op jit(solution)/shard_map/dot_general | solution.py:192
  (132 shorter events, 46.6 us)
Async XLA Ops:
  0.0 25.2 %copy-start = (bf16[2048,128]{1,0:T(8,128)(2,1)S(1)}, bf16[2048,128]{1,0:T(8,128)(2,1)}, u32[]{:S(2)}) copy-start(bf16[2048,128]{1,0:T(8,128)(2,1)} %param.12) | copy-start | bytes 1572868
  25.2 6.4 %copy-start.7 = (bf16[2048,128]{1,0:T(8,128)(2,1)S(1)}, bf16[2048,128]{1,0:T(8,128)(2,1)}, u32[]{:S(2)}) copy-start(bf16[2048,128]{1,0:T(8,128)(2,1)} %param.13) | copy-start | bytes 1572868
  48.1 1.0 copy-start.4
  82.0 10.6 %copy-start.8 = (bf16[2048,128]{1,0:T(8,128)(2,1)S(1)}, bf16[2048,128]{1,0:T(8,128)(2,1)}, u32[]{:S(2)}) copy-start(bf16[2048,128]{1,0:T(8,128)(2,1)} %param.16) | copy-start | bytes 1572868
  84.5 27.4 %all-to-all-start = ((f32[16,129,128]{2,1,0:T(8,128)}), f32[16,129,128]{2,1,0:T(8,128)}, u32[]{:S(2)}, u32[]{:S(2)}) async-start(f32[16,129,128]{2,1,0:T(8,128)} %broadcast_in_dim.58), calls=%async_computation | async-start | bytes 2228224 | tf_op jit(solution)/shard_map/all_to_all | solution.py:32
  92.6 9.6 %copy-start.6 = (bf16[2048,1,64]{0,2,1:T(8,128)(2,1)S(1)}, bf16[2048,1,64]{0,2,1:T(8,128)(2,1)}, u32[]{:S(2)}) copy-start(bf16[2048,1,64]{0,2,1:T(8,128)(2,1)} %get-tuple-element.78) | copy-start | bytes 786436
  98.4 8.7 %copy-start.2 = (bf16[2048,128]{1,0:T(8,128)(2,1)}, bf16[2048,128]{1,0:T(8,128)(2,1)S(1)}, u32[]{:S(2)}) copy-start(bf16[2048,128]{1,0:T(8,128)(2,1)S(1)} %convolution_convert_fusion) | copy-start | bytes 1572868
  98.4 8.5 %collective-permute-start = (bf16[15,128]{1,0:T(8,128)(2,1)S(1)}, bf16[15,128]{1,0:T(8,128)(2,1)S(1)}, u32[]{:S(2)}, u32[]{:S(2)}) collective-permute-start(bf16[15,128]{1,0:T(8,128)(2,1)S(1)} %slice.158), channel_id=1, source_target_pairs={{0,8},{8,16},{16,24},{24,32},{32,40},{40,48},{48,56},{56,64},{64,7... | collective-permute-start | bytes 11528 | tf_op jit(solution)/shard_map/ppermute | solution.py:27
  108.1 1.0 copy-start.3
  111.9 24.0 %all-to-all-start.2 = ((bf16[8,256,128]{1,2,0:T(8,128)(2,1)}), bf16[8,256,128]{1,2,0:T(8,128)(2,1)}, u32[]{:S(2)}, u32[]{:S(2)}) async-start(bf16[8,256,128]{1,2,0:T(8,128)(2,1)} %copy.46), calls=%async_computation.2 | async-start | bytes 1048576 | tf_op jit(solution)/shard_map/all_to_all | solution.py:190
  118.0 2.4 %copy-start.1 = (bf16[2048,1,64]{2,0,1:T(8,128)(2,1)S(1)}, bf16[2048,1,64]{2,0,1:T(8,128)(2,1)}, u32[]{:S(2)}) copy-start(bf16[2048,1,64]{2,0,1:T(8,128)(2,1)} %copy.49) | copy-start | bytes 786436
  118.0 2.4 %copy-start.5 = (f32[16,1,128,128]{3,2,1,0:T(8,128)S(1)}, f32[16,1,128,128]{3,2,1,0:T(8,128)}, u32[]{:S(2)}) copy-start(f32[16,1,128,128]{3,2,1,0:T(8,128)} %get-tuple-element.33) | copy-start | bytes 3145732
  122.0 3.0 %copy-start.9 = (f32[128]{0:T(128)S(1)}, f32[128]{0:T(128)}, u32[]{:S(2)}) copy-start(f32[128]{0:T(128)} %param.17) | copy-start | bytes 1540
  135.9 15.1 %all-to-all-start.1 = ((bf16[8,256,128]{2,1,0:T(8,128)(2,1)}), bf16[8,256,128]{2,1,0:T(8,128)(2,1)S(1)}, u32[]{:S(2)}, u32[]{:S(2)}) async-start(bf16[8,256,128]{2,1,0:T(8,128)(2,1)} %fusion.65), calls=%async_computation.1 | async-start | bytes 1048576 | tf_op jit(solution)/shard_map/all_to_all | solution.py:17
